TPU v7x, 32 devices: a whole 2x2x4 slice. The times are simulated.
32 devices in a mesh: sp: 8 (over z, y), tp: 4 (over x, core).
Axes of the slice: x: 2, y: 2, z: 4, core: 2. Of those that a mesh axis runs over, the one named last changes fastest.
Arguments:
- latent: bfloat16 [2048, 2048], P(('sp', 'tp')), may hold values from -6 to 6
- log_decay: float32 [2048, 8], P('sp', 'tp'), may hold values from -2 to 0
- context: bfloat16 [128, 2048], P('sp'), may hold values from -6 to 6
- condition: bfloat16 [2, 2048], replicated, may hold values from -6 to 6
- w_modulate: bfloat16 [2048, 6144], P('sp', 'tp'), may hold values from -1 to 1
- norm_gain: bfloat16 [2048], replicated, may hold values from 0.099609375 to 1.8984375
- w_query: bfloat16 [2048, 2048], P(None, 'tp'), may hold values from -0.125 to 0.125
- w_key: bfloat16 [2048, 2048], P(None, 'tp'), may hold values from -0.125 to 0.125
- w_value: bfloat16 [2048, 4096], P(None, 'tp'), may hold values from -0.125 to 0.125
- w_gate: bfloat16 [2048, 4096], P(None, 'tp'), may hold values from -0.125 to 0.125
- group_gain: bfloat16 [4096], P('tp'), may hold values from 0.099609375 to 1.8984375
- w_output: bfloat16 [4096, 2048], P('tp'), may hold values from -0.125 to 0.125
Outputs:
- updated: bfloat16 [2048, 2048], P(('sp', 'tp'))
All inputs are finite; a program needn't handle non-finite values.
Results may differ from a plain program's by a relative error of at most 0.014.
Values may be sent and summed in bfloat16 or wider, within the bound.
A program may use at most 128 MiB of HBM per device.

v0:
```python
import jax
import jax.numpy as jnp
from jax import lax
from jax.sharding import PartitionSpec as P

DK = 256
DV = 512
BLOCK = 128
GRID_W = 64
CTX_LIFT = 4


epsilon = 1e-06
rotary_base = 10000.0


def carried_in_2(array, axis, combine, identity, reverse):
    size, here = (lax.axis_size(axis), lax.axis_index(axis))
    everything = jax.tree.map(lambda part: lax.all_gather(part, axis), array)
    start = jax.tree.map(
        lambda part, zero: jnp.broadcast_to(jnp.asarray(zero, part.dtype), part.shape),
        array,
        identity,
    )

    def hop(k, before):
        at = size - 1 - k if reverse else k
        reached = at > here if reverse else at < here
        new = combine(before, jax.tree.map(lambda part: part[at], everything))
        return jax.tree.map(lambda a, b: jnp.where(reached, a, b), new, before)

    return lax.fori_loop(0, size, hop, start)


def modulate_rows(row_block, norm_gain, shift_vec, scale_vec):
    wide = row_block.astype(jnp.float32)
    normal = wide * lax.rsqrt(jnp.mean(wide * wide, axis=-1, keepdims=True) + epsilon)
    return (normal * norm_gain.astype(jnp.float32) * (1.0 + scale_vec) + shift_vec).astype(
        jnp.bfloat16
    )


def rotate(projected, positions):
    pairs = DK // 4
    inverse = rotary_base ** (-jnp.arange(pairs, dtype=jnp.float32) / pairs)
    grid_row = (positions // GRID_W).astype(jnp.float32)
    grid_column = (positions % GRID_W).astype(jnp.float32)
    angles = jnp.concatenate([grid_row[:, None] * inverse, grid_column[:, None] * inverse], axis=-1)
    cosine = jnp.cos(angles)[:, None, :]
    sine_part = jnp.sin(angles)[:, None, :]
    paired = projected.reshape(projected.shape[0], -1, DK // 2, 2)
    even_part = paired[..., 0]
    odd_part = paired[..., 1]
    turned = jnp.stack(
        [even_part * cosine - odd_part * sine_part, even_part * sine_part + odd_part * cosine],
        axis=-1,
    )
    return turned.reshape(projected.shape)


def context_terms(normal_rows, w_key, w_value):
    head_count = w_key.shape[1] // DK
    key_part = (
        jnp.dot(normal_rows, w_key, preferred_element_type=jnp.float32) * DK ** (-0.5)
    ).astype(jnp.bfloat16)
    value_part = jnp.dot(normal_rows, w_value, preferred_element_type=jnp.float32).astype(
        jnp.bfloat16
    )
    return jnp.einsum(
        "jhd,jhv->hdv",
        key_part.reshape(-1, head_count, DK),
        value_part.reshape(-1, head_count, DV),
        preferred_element_type=jnp.float32,
    )


def block_pass(queries, key_rows, value_rows, decays):
    block_count = queries.shape[0] // BLOCK
    head_count = queries.shape[1]
    query_blocks = queries.reshape(block_count, BLOCK, head_count, DK)
    key_blocks = key_rows.reshape(block_count, BLOCK, head_count, DK)
    value_blocks = value_rows.reshape(block_count, BLOCK, head_count, DV)
    cumulative = jnp.cumsum(decays.reshape(block_count, BLOCK, head_count), axis=1)
    by_head = jnp.swapaxes(cumulative, 1, 2)
    within = jnp.arange(BLOCK, dtype=jnp.int32)
    lower_mask = within[:, None] >= within[None, :]
    log_gaps = by_head[:, :, :, None] - by_head[:, :, None, :]
    weights = jnp.where(lower_mask, jnp.exp(jnp.where(lower_mask, log_gaps, 0.0)), 0.0)
    scores = jnp.einsum(
        "nihd,njhd->nhij", query_blocks, key_blocks, preferred_element_type=jnp.float32
    )
    weighted = (scores * weights).astype(jnp.bfloat16)
    inside = jnp.einsum(
        "nhij,njhv->nihv", weighted, value_blocks, preferred_element_type=jnp.float32
    )
    totals = cumulative[:, -1, :]
    decayed = (
        key_blocks.astype(jnp.float32) * jnp.exp(totals[:, None, :] - cumulative)[..., None]
    ).astype(jnp.bfloat16)
    updates = jnp.einsum(
        "njhd,njhv->nhdv", decayed, value_blocks, preferred_element_type=jnp.float32
    )
    return (query_blocks, cumulative, inside, totals, updates)


def fold_blocks(totals, updates):

    def fold_advance(carried, element):
        log_total, states = carried
        block_total, block_update = element
        return (
            (log_total + block_total, jnp.exp(block_total)[:, None, None] * states + block_update),
            None,
        )

    initial = (jnp.zeros(totals.shape[1:], jnp.float32), jnp.zeros(updates.shape[1:], jnp.float32))
    result, unused = lax.scan(fold_advance, initial, (totals, updates))
    return result


def link_states(earlier, later):
    return (earlier[0] + later[0], jnp.exp(later[0])[:, None, None] * earlier[1] + later[1])


def finish_pass(query_blocks, cumulative, inside, totals, updates, entry):

    def finish_advance(states, element):
        block_total, block_update = element
        return (jnp.exp(block_total)[:, None, None] * states + block_update, states)

    unused, entering = lax.scan(finish_advance, entry, (totals, updates))
    carried_in = jnp.exp(cumulative)[..., None] * jnp.einsum(
        "nihd,nhdv->nihv",
        query_blocks,
        entering.astype(jnp.bfloat16),
        preferred_element_type=jnp.float32,
    )
    combined = inside + carried_in
    return combined.reshape(-1, combined.shape[2], combined.shape[3])


def enter_state(prefix, context_state):
    return jnp.exp(prefix[0])[:, None, None] * context_state + prefix[1]


def per_device(
    latent,
    log_decay,
    context,
    condition,
    w_modulate,
    norm_gain,
    w_query,
    w_key,
    w_value,
    w_gate,
    group_gain,
    w_output,
):
    head_devices = lax.axis_size("tp")
    seq_index = lax.axis_index("sp")
    model_width = latent.shape[1]
    head_count = w_query.shape[1] // DK
    activated = jax.nn.silu(condition.astype(jnp.float32)).astype(jnp.bfloat16)
    input_rows = w_modulate.shape[0]
    own_inputs = lax.dynamic_slice_in_dim(activated, seq_index * input_rows, input_rows, 1)
    partial_mod = jnp.dot(own_inputs, w_modulate, preferred_element_type=jnp.float32)
    summed = lax.psum(partial_mod, "sp")
    modulation = lax.all_gather(summed, "tp", axis=1, tiled=True)
    latent_shift = modulation[0, :model_width]
    latent_scale = modulation[0, model_width : 2 * model_width]
    latent_gate = modulation[0, 2 * model_width :]
    context_shift = modulation[1, :model_width]
    context_scale = modulation[1, model_width : 2 * model_width]
    normed = modulate_rows(latent, norm_gain, latent_shift, latent_scale)
    row_base = seq_index * (latent.shape[0] * head_devices)
    key_width = w_query.shape[1]
    value_width = w_value.shape[1]
    shard_rows = lax.all_gather(normed, "tp", axis=0, tiled=True)
    positions = row_base + jnp.arange(shard_rows.shape[0], dtype=jnp.int32)
    query_part = rotate(jnp.dot(shard_rows, w_query, preferred_element_type=jnp.float32), positions)
    key_part = rotate(
        jnp.dot(shard_rows, w_key, preferred_element_type=jnp.float32), positions
    ) * DK ** (-0.5)
    value_part = jnp.dot(shard_rows, w_value, preferred_element_type=jnp.float32)
    gate_part = jnp.dot(shard_rows, w_gate, preferred_element_type=jnp.float32)
    projected = jnp.concatenate([query_part, key_part, value_part, gate_part], axis=1).astype(
        jnp.bfloat16
    )
    row_total = projected.shape[0]
    query_rows = projected[:, :key_width].reshape(row_total, head_count, DK)
    key_rows = projected[:, key_width : 2 * key_width].reshape(row_total, head_count, DK)
    value_rows = projected[:, 2 * key_width : 2 * key_width + value_width].reshape(
        row_total, head_count, DV
    )
    gate_rows = projected[:, 2 * key_width + value_width :]
    empty_state = jnp.zeros((head_count, DK, DV), jnp.float32)
    context_sum = context_terms(
        modulate_rows(
            lax.all_gather(context, "sp", axis=0, tiled=True),
            norm_gain,
            context_shift,
            context_scale,
        ),
        w_key,
        w_value,
    )
    context_state = context_sum * float(CTX_LIFT)
    forward_parts = block_pass(query_rows, key_rows, value_rows, log_decay)
    backward_parts = block_pass(
        jnp.flip(query_rows, 0),
        jnp.flip(key_rows, 0),
        jnp.flip(value_rows, 0),
        jnp.flip(log_decay, 0),
    )
    identity = (jnp.zeros((head_count,), jnp.float32), empty_state)
    earlier_blocks = carried_in_2(
        fold_blocks(forward_parts[3], forward_parts[4]), "sp", link_states, identity, False
    )
    later_blocks = carried_in_2(
        fold_blocks(backward_parts[3], backward_parts[4]), "sp", link_states, identity, True
    )
    forward = finish_pass(*forward_parts, enter_state(earlier_blocks, context_state))
    backward = jnp.flip(finish_pass(*backward_parts, enter_state(later_blocks, context_state)), 0)
    mixed_heads = forward + backward
    average = jnp.mean(mixed_heads, axis=-1, keepdims=True)
    variance = jnp.mean(jnp.square(mixed_heads - average), axis=-1, keepdims=True)
    normal_heads = ((mixed_heads - average) * lax.rsqrt(variance + epsilon)).reshape(
        row_total, head_count * DV
    )
    attended = (
        jax.nn.silu(gate_rows.astype(jnp.float32)) * normal_heads * group_gain.astype(jnp.float32)
    ).astype(jnp.bfloat16)
    projected_sum = lax.psum_scatter(
        jnp.dot(attended, w_output, preferred_element_type=jnp.float32).astype(jnp.bfloat16),
        "tp",
        scatter_dimension=0,
        tiled=True,
    ).astype(jnp.float32)
    return (latent.astype(jnp.float32) + latent_gate * projected_sum).astype(jnp.bfloat16)


def solution(mesh):
    placed = (
        P(("sp", "tp"), None),
        P("sp", "tp"),
        P("sp", None),
        P(),
        P("sp", "tp"),
        P(),
        P(None, "tp"),
        P(None, "tp"),
        P(None, "tp"),
        P(None, "tp"),
        P("tp"),
        P("tp", None),
    )
    return jax.shard_map(
        per_device, mesh=mesh, in_specs=placed, out_specs=P(("sp", "tp"), None), check_vma=False
    )
```

profile of v0, /device:TPU:0, one launch (start us, length us, event | category | flops | bytes accessed | tf_op | source)
XLA Modules:
  0.0 443.5 jit_solution(4623443041983186782)
XLA Ops:
  8.7 38.9 %psum.7 = f32[2,1536]{1,0:T(2,128)S(1)} all-reduce(f32[2,1536]{1,0:T(2,128)S(1)} %fusion.76), channel_id=1, replica_groups=mesh['sp'=8,'tp'=4] {'sp'}, use_global_device_ids=true, to_apply=%region_0.1 | all-reduce | flops 3072 | bytes 24576 | tf_op jit(solution)/shard_map/psum | solution.py:168
  47.6 5.2 %all_gather.33 = f32[2,6144]{1,0:T(2,128)S(1)} all-gather(f32[2,1536]{1,0:T(2,128)S(1)} %psum.7), channel_id=1, replica_groups=mesh['sp'=8,'tp'=4] {'tp'}, dimensions={1}, use_global_device_ids=true | all-gather | bytes 61440 | tf_op jit(solution)/shard_map/all_gather | solution.py:169
  61.0 10.2 %all-gather.8.cloned.1.call-done = bf16[256,2048]{1,0:T(8,128)(2,1)} async-done(((bf16[64,2048]{1,0:T(8,128)(2,1)}), bf16[256,2048]{1,0:T(8,128)(2,1)}) %all-gather.8.cloned.1.call-update) | async-done | bytes 1048592 | tf_op jit(solution)/shard_map/all_gather | solution.py:179
  71.2 3.7 fusion.91
  77.0 3.0 fusion.92
  82.1 3.7 subtract_convert_fusion
  90.7 3.8 convolution_convert_fusion.1
  96.1 8.4 %rev.19 = bf16[256,2,512]{2,0,1:T(8,128)(2,1)} reverse(bf16[256,2,512]{2,0,1:T(8,128)(2,1)} %bitcast.157), dimensions={0} | reverse | bytes 1048576 | tf_op jit(solution)/shard_map/jit(_flip)/rev | solution.py:213
  104.5 3.0 fusion.37
  107.5 3.1 while.88
  124.0 2.8 fusion.40
  126.8 4.9 %while.86 = (s32[]{:T(128)}, f32[2]{0:T(128)}, f32[2,256,512]{2,1,0:T(8,128)S(1)}, f32[2,2]{1,0:T(2,128)S(1)}, f32[2,2,256,512]{3,2,1,0:T(8,128)}, /*index=5*/s32[]{:T(128)}, s32[]{:T(128)}) while((s32[]{:T(128)}, f32[2]{0:T(128)}, f32[2,256,512]{2,1,0:T(8,128)S(1)}, f32[2,2]{1,0:T(2,128)S(1)}, f32[2,2,256,512]{3,2,1,0:T(8,128)}, ...), condition=%wide.region_5.6_spmd.clone, body=%wide.region_4.5_spmd.clone.sunk | while | flops 786439 | bytes 3145864 | solution.py:117
  132.9 33.8 %all_gather.35 = bf16[128,2048]{1,0:T(8,128)(2,1)S(1)} all-gather(bf16[16,2048]{1,0:T(8,128)(2,1)} %param.26), channel_id=1, replica_groups=mesh['sp'=8,'tp'=4] {'sp'}, dimensions={0}, use_global_device_ids=true | all-gather | bytes 589824 | tf_op jit(solution)/shard_map/all_gather | solution.py:200
  178.4 3.9 convolution_convert_fusion.3
  183.4 22.6 %all-reduce.2 = (f32[16]{0:T(128)S(1)}, f32[16]{0:T(128)S(1)}) all-reduce(f32[16]{0:T(128)S(1)} %dynamic-update-slice.1, f32[16]{0:T(128)S(1)} %dynamic-update-slice), channel_id=4, replica_groups=mesh['sp'=8,'tp'=4] {'sp'}, use_global_device_ids=true, to_apply=%add.1 | all-reduce | flops 32 | bytes 256
  210.4 31.1 %all-gather.12.cloned.1.call-done = f32[16,256,512]{2,1,0:T(8,128)} async-done(((f32[2,256,512]{2,1,0:T(8,128)}), f32[16,256,512]{2,1,0:T(8,128)}) %all-gather.12.cloned.1.call-update) | async-done | bytes 8388624 | tf_op jit(solution)/shard_map/all_gather | solution.py:19
  241.6 13.6 %while.89 = (s32[]{:T(128)}, f32[2]{0:T(128)S(1)}, f32[2,256,512]{2,1,0:T(8,128)S(1)}, s32[]{:T(128)}, f32[8,2]{1,0:T(8,128)S(1)}, /*index=5*/f32[8,2,256,512]{3...) while((s32[]{:T(128)}, f32[2]{0:T(128)S(1)}, f32[2,256,512]{2,1,0:T(8,128)S(1)}, ...), condition=%wide.region_14.15_spmd.clone, body=%wide.region_13.14_spmd.clone.sunk | while | flops 1048590 | bytes 3145945 | solution.py:32
  255.7 110.6 %all-gather.10.cloned.1.call-done = f32[16,256,512]{2,1,0:T(8,128)} async-done(((f32[2,256,512]{2,1,0:T(8,128)}), f32[16,256,512]{2,1,0:T(8,128)}) %all-gather.10.cloned.1.call-update) | async-done | bytes 8388624 | tf_op jit(solution)/shard_map/all_gather | solution.py:19
  366.4 13.3 %while.87 = (s32[]{:T(128)}, f32[2]{0:T(128)S(1)}, f32[2,256,512]{2,1,0:T(8,128)S(1)}, s32[]{:T(128)}, f32[8,2]{1,0:T(8,128)S(1)}, /*index=5*/f32[8,2,256,512]{3,2,1,0:T(8,128)}, s32[]{:T(128)}, s32[]{:T(128)}) while((s32[]{:T(128)}, f32[2]{0:T(128)S(1)}, f32[2,256,512]{2,1,0:T(8,128)S(1)}, s32[]{:T(128)}, f32[8,2]{1,0:T(8,128)S(1)}, ...), condition=%wide.region_7.8_spmd.clone, body=%wide.region_6.7_spmd.clone.sunk | while | flops 1048586 | bytes 3145883 | solution.py:32
  382.4 6.1 %while.84 = (s32[]{:T(128)}, f32[2,256,512]{2,1,0:T(8,128)S(1)}, bf16[2,2,256,512]{3,2,1,0:T(8,128)(2,1)}, f32[2,2]{1,0:T(2,128)}, f32[2,2,256,512]{3,2,1,0:T(8,128)}, /*index=5*/s32[]{:T(128)}) while((s32[]{:T(128)}, f32[2,256,512]{2,1,0:T(8,128)S(1)}, bf16[2,2,256,512]{3,2,1,0:T(8,128)(2,1)}, f32[2,2]{1,0:T(2,128)}, ...), condition=%wide.region_9.10_spmd, body=%wide.region_8.9_spmd.sunk | while | flops 524290 | bytes 5243493 | solution.py:131
  394.0 4.9 %while.85 = (s32[]{:T(128)}, f32[2,256,512]{2,1,0:T(8,128)S(1)}, bf16[2,2,256,512]{3,2,1,0:T(8,128)(2,1)}, f32[2,2]{1,0:T(2,128)S(1)}, f32[2,2,256,512]{3,2,1,0:T(8,128)}, /*index=5*/s32[]{:T(128)}) while((s32[]{:T(128)}, f32[2,256,512]{2,1,0:T(8,128)S(1)}, bf16[2,2,256,512]{3,2,1,0:T(8,128)(2,1)}, f32[2,2]{1,0:T(2,128)S(1)}, ...), condition=%wide.region_16.17_spmd, body=%wide.region_15.16_spmd.sunk | while | flops 524290 | bytes 5243493 | solution.py:131
  398.9 2.5 fusion.11
  404.7 7.4 %convolution_convert_fusion = bf16[256,2048]{1,0:T(8,128)(2,1)} fusion(bf16[1024,2048]{1,0:T(8,128)(2,1)} %param.35, f32[256,1024]{1,0:T(8,128)S(1)} %bitcast.160, bf16[256,2048]{1,0:T(8,128)(2,1)} %all-gather.8.cloned.1.call-done, bf16[2048,1024]{1,0:T(8,128)(2,1)} %param.33, f32[1024]{0:T(1024)S(1)} %copy-done.32), kind=kOutput, calls=%fused_computation.34 | convolution fusion | flops 2150367232 | bytes 11538432 | tf_op jit(solution)/shard_map/dot_general | solution.py:235
  412.0 23.2 %reduce-scatter.2.cloned.1.call-done = bf16[64,2048]{1,0:T(8,128)(2,1)} async-done(((bf16[256,2048]{1,0:T(8,128)(2,1)}), bf16[64,2048]{1,0:T(8,128)(2,1)}) %reduce-scatter.2.cloned.1.call-update) | async-done | bytes 262160 | tf_op jit(solution)/shard_map/reduce_scatter | solution.py:234
  (211 shorter events, 111.0 us)
Async XLA Ops:
  6.5 70.5 %copy-start = (bf16[2048,512]{1,0:T(8,128)(2,1)S(1)}, bf16[2048,512]{1,0:T(8,128)(2,1)}, u32[]{:S(2)}) copy-start(bf16[2048,512]{1,0:T(8,128)(2,1)} %param.31) | copy-start | bytes 6291460
  6.5 64.7 %all-gather.8.cloned.1.call-start = ((), (), s32[]{:S(2)}) async-start(), calls=%async_computation.1 | async-start | bytes 1310720 | tf_op jit(solution)/shard_map/all_gather | solution.py:179
  54.1 112.7 %copy-start.19 = (f32[2048]{0:T(1024)}, f32[2048]{0:T(1024)S(1)}, u32[]{:S(2)}) copy-start(f32[2048]{0:T(1024)S(1)} %convert_element_type.91) | copy-start | bytes 24580
  57.1 184.4 %all-gather.12.cloned.1.call-start = ((), (), s32[]{:S(2)}) async-start(), calls=%async_computation.4 | async-start | bytes 9437184 | tf_op jit(solution)/shard_map/all_gather | solution.py:19
  110.6 16.2 %copy-start.20 = (f32[2,2]{1,0:T(2,128)}, f32[2,2]{1,0:T(2,128)S(1)}, u32[]{:S(2)}) copy-start(f32[2,2]{1,0:T(2,128)S(1)} %get-tuple-element.928) | copy-start | bytes 52
  111.6 254.7 %all-gather.10.cloned.1.call-start = ((), (), s32[]{:S(2)}) async-start(), calls=%async_computation.3 | async-start | bytes 9437184 | tf_op jit(solution)/shard_map/all_gather | solution.py:19
  131.8 45.9 %copy-start.22 = (f32[2,2]{1,0:T(2,128)}, f32[2,2]{1,0:T(2,128)S(1)}, u32[]{:S(2)}) copy-start(f32[2,2]{1,0:T(2,128)S(1)} %get-tuple-element.929) | copy-start | bytes 52
  132.8 302.4 %reduce-scatter.2.cloned.1.call-start = ((), (), s32[]{:S(2)}) async-start(), calls=%async_computation.2 | async-start | bytes 1310720 | tf_op jit(solution)/shard_map/reduce_scatter | solution.py:234
  169.3 13.0 %copy-start.29 = (f32[2]{0:T(128)S(1)}, f32[2]{0:T(128)}, u32[]{:S(2)}) copy-start(f32[2]{0:T(128)} %get-tuple-element.380) | copy-start | bytes 28
  169.3 13.3 %copy-start.28 = (f32[2]{0:T(128)S(1)}, f32[2]{0:T(128)}, u32[]{:S(2)}) copy-start(f32[2]{0:T(128)} %copy-done.27) | copy-start | bytes 28
  169.3 13.5 %copy-start.33 = (bf16[1024]{0:T(1024)(128)(2,1)S(1)}, bf16[1024]{0:T(1024)(128)(2,1)}, u32[]{:S(2)}) copy-start(bf16[1024]{0:T(1024)(128)(2,1)} %param.34) | copy-start | bytes 6148
  169.3 36.6 %copy-start.15 = (bf16[256,2,128,1]{0,3,2,1:T(2,128)(2,1)S(1)}, bf16[256,2,128,1]{0,3,2,1:T(2,128)(2,1)}, u32[]{:S(2)}) copy-start(bf16[256,2,128,1]{0,3,2,1:T(2,128)(2,1)} %get-tuple-element.544) | copy-start | bytes 393220
  169.3 36.6 %copy-start.16 = (bf16[256,2,128,1]{0,3,2,1:T(2,128)(2,1)S(1)}, bf16[256,2,128,1]{0,3,2,1:T(2,128)(2,1)}, u32[]{:S(2)}) copy-start(bf16[256,2,128,1]{0,3,2,1:T(2,128)(2,1)} %get-tuple-element.545) | copy-start | bytes 393220
  178.4 63.2 %copy-start.4 = (f32[2,256,512]{2,1,0:T(8,128)S(1)}, f32[2,256,512]{2,1,0:T(8,128)}, u32[]{:S(2)}) copy-start(f32[2,256,512]{2,1,0:T(8,128)} %custom-call.7) | copy-start | bytes 3145732
  178.4 63.2 %copy-start.26 = (f32[2]{0:T(128)S(1)}, f32[2]{0:T(128)}, u32[]{:S(2)}) copy-start(f32[2]{0:T(128)} %custom-call.6) | copy-start | bytes 28
  241.6 124.8 %copy-start.25 = (f32[2]{0:T(128)S(1)}, f32[2]{0:T(128)}, u32[]{:S(2)}) copy-start(f32[2]{0:T(128)} %custom-call.2) | copy-start | bytes 28
  255.1 111.3 %copy-start.5 = (f32[2,256,512]{2,1,0:T(8,128)}, f32[2,256,512]{2,1,0:T(8,128)S(1)}, u32[]{:S(2)}) copy-start(f32[2,256,512]{2,1,0:T(8,128)S(1)} %get-tuple-element.388) | copy-start | bytes 3145732
  366.4 13.4 %copy-start.17 = (bf16[128,512]{0,1:T(8,128)(2,1)S(1)}, bf16[128,512]{0,1:T(8,128)(2,1)}, u32[]{:S(2)}) copy-start(bf16[128,512]{0,1:T(8,128)(2,1)} %copy.95) | copy-start | bytes 393220
  382.4 7.8 %copy-start.7 = (bf16[2,128,2,512]{3,2,1,0:T(2,128)(2,1)S(1)}, bf16[2,128,2,512]{3,2,1,0:T(2,128)(2,1)}, u32[]{:S(2)}) copy-start(bf16[2,128,2,512]{3,2,1,0:T(2,128)(2,1)} %reshape_reshape.9) | copy-start | bytes 1572868
  382.4 7.8 %copy-start.9 = (bf16[2,128,2,256]{1,0,3,2:T(2,128)(2,1)S(1)}, bf16[2,128,2,256]{1,0,3,2:T(2,128)(2,1)}, u32[]{:S(2)}) copy-start(bf16[2,128,2,256]{1,0,3,2:T(2,128)(2,1)} %reshape_reshape.11) | copy-start | bytes 786436
  382.4 7.8 %copy-start.24 = (f32[2,2,128]{2,1,0:T(2,128)S(1)}, f32[2,2,128]{2,1,0:T(2,128)}, u32[]{:S(2)}) copy-start(f32[2,2,128]{2,1,0:T(2,128)} %copy.62) | copy-start | bytes 6148
  404.6 30.5 %copy-start.8 = (bf16[64,2048]{1,0:T(8,128)(2,1)S(1)}, bf16[64,2048]{1,0:T(8,128)(2,1)}, u32[]{:S(2)}) copy-start(bf16[64,2048]{1,0:T(8,128)(2,1)} %param.24) | copy-start | bytes 786436
  404.6 30.5 %copy-start.18 = (f32[1,2048]{1,0:T(1,128)S(1)}, f32[1,2048]{1,0:T(1,128)}, u32[]{:S(2)}) copy-start(f32[1,2048]{1,0:T(1,128)} %get-tuple-element.556) | copy-start | bytes 24580
  404.6 32.3 %copy-start.1 = (bf16[2048,512]{1,0:T(8,128)(2,1)S(1)}, bf16[2048,512]{1,0:T(8,128)(2,1)}, u32[]{:S(2)}) copy-start(bf16[2048,512]{1,0:T(8,128)(2,1)} %param.31) | copy-start | bytes 6291460
  (15 other events, 50.6 us)
Sparse Core Ops, SparseCore 0:
  57.2 13.9 all-gather.7
  111.8 129.7 all-gather.11
  243.7 122.6 all-gather.9
  412.1 22.9 reduce-scatter.1
where the time goes:
time: 446 us; the launch traced here: 443 us
  waiting for transfers between devices  175 us (39%)
  blocking collectives  100 us (22%)
  other arithmetic  61 us (14%)
  local copies, waits for them, and re-layouts  52.4 us (12%)
  matrix products  39.5 us (9%)
  between operations  14.3 us (3%)
    all_gather x2, waiting for transfers between devices, carried_in_2(): everything = jax.tree.map(lambda part: lax.all_gather(part, axis), array)  142 us
    psum x1, blocking collectives, per_device(): summed = lax.psum(partial_mod, 'sp')  38.9 us
    all_gather x1, blocking collectives, per_device(): lax.all_gather(context, 'sp', axis=0, tiled=True)  33.8 us
    select_n x16, other arithmetic, hop(): return jax.tree.map(lambda a, b: jnp.where(reached, a, b), new, before)  26.1 us
    reduce_scatter x1, waiting for transfers between devices, per_device(): lax.psum_scatter(jnp.dot(attended, w_output, preferred_element_type=jnp.f...  23.2 us
    unnamed x1, blocking collectives  22.6 us
    all_gather x1, waiting for transfers between devices, per_device(): shard_rows = lax.all_gather(normed, 'tp', axis=0, tiled=True)  10.2 us
  transfers between devices with their start and end apart: 4, of which 4 were waited for; matrix products, arithmetic and copies ran while one was open for 13% of the time, Pallas kernels for 0%

commit v1 on v0

v1 whole, which is shorter than its diff:
```python
import functools

import jax
import jax.numpy as jnp
import numpy as np
from jax import lax
from jax.experimental import pallas as pl
from jax.experimental.pallas import tpu as pltpu
from jax.sharding import PartitionSpec as P

DK = 256
DV = 512
GRID_W = 64
CTX_LIFT = 4
CORES = 2
CHUNKS = 4

epsilon = 1e-06
rotary_base = 10000.0
MESH = pl.DeviceIdType.MESH
F32 = jnp.float32
BF16 = jnp.bfloat16


def silu(v):
    return v / (1.0 + jnp.exp(-v))


def rotary_tables(grid_rows):
    pairs = DK // 4
    inverse = (rotary_base ** (-np.arange(pairs, dtype=np.float64) / pairs)).astype(np.float32)

    def tables(count):
        angles = (np.arange(count, dtype=np.float32)[:, None] * inverse[None, :]).astype(np.float32)
        cosine = np.repeat(np.cos(angles.astype(np.float64)), 2, axis=1)
        sine = np.repeat(np.sin(angles.astype(np.float64)), 2, axis=1)
        sine[:, 0::2] *= -1.0
        return cosine.astype(np.float32), sine.astype(np.float32)

    return tables(grid_rows) + tables(GRID_W)


def kernel(
    n_sp, n_tp, group, rows, head_count,
    lat_ref, dec_ref, ctx_ref, cond_ref, ngain_ref, ggain_ref,
    rowc_ref, rows_ref, colc_ref, cols_ref,
    wmod_hbm, wq_hbm, wk_hbm, wv_hbm, wg_hbm, wo_hbm,
    out_ref,
    wmod, wk, wv, wq, wg, wo,
    lat_all, normed, ctx_all, dec_all, mslots, modfull,
    wdec, vecs, etot,
    kbuf, qbuf, vbuf, gbuf, ybuf, fstate, bstate,
    recv_f, recv_b, send_f, send_b,
    att, pout, pin, psend, pfin,
    w_sem, dec_s, dec_r, m1_s, m1_r, m2_s, m2_r, lat_s, lat_r, rel_s, rel_r,
    ctx_s, ctx_r, f_s, f_r, b_s, b_r, d2d_s, d2d_r, ici_s, ici_r,
):
    sp = lax.axis_index("sp")
    tp = lax.axis_index("tp")
    zz = sp // group
    sub = sp % group
    nz = n_sp // group
    members = group * n_tp
    chips = members // CORES
    me = sub * n_tp + tp
    chip = me // CORES
    core = me % CORES
    tokens = members * rows
    model = lat_ref.shape[1]

    def member_device(m):
        return (zz * group + m // n_tp, m % n_tp)

    partner = member_device(chip * CORES + (1 - core))

    def remote(src, dst, ssem, rsem, device):
        return pltpu.make_async_remote_copy(
            src_ref=src, dst_ref=dst, send_sem=ssem, recv_sem=rsem,
            device_id=device, device_id_type=MESH,
        )

    key_cols = pl.ds(pl.multiple_of(sub * DK, DK), DK)
    val_cols = pl.ds(pl.multiple_of(sub * DV, DV), DV)
    loads = [
        pltpu.make_async_copy(wmod_hbm, wmod, w_sem.at[0]),
        pltpu.make_async_copy(wk_hbm.at[:, key_cols], wk, w_sem.at[1]),
        pltpu.make_async_copy(wv_hbm.at[:, val_cols], wv, w_sem.at[2]),
        pltpu.make_async_copy(wq_hbm.at[:, key_cols], wq, w_sem.at[3]),
        pltpu.make_async_copy(wg_hbm.at[:, val_cols], wg, w_sem.at[4]),
        pltpu.make_async_copy(wo_hbm.at[val_cols, :], wo, w_sem.at[5]),
    ]
    for load in loads:
        load.start()

    barrier = pltpu.get_barrier_semaphore()
    greeted = 0
    for d in range(1, n_sp):
        pl.semaphore_signal(
            barrier, inc=1, device_id=((sp + d) % n_sp, tp), device_id_type=MESH
        )
        greeted += 1
    for s in range(group):
        for d in range(1, n_tp):
            pl.semaphore_signal(
                barrier, inc=1, device_id=(zz * group + s, (tp + d) % n_tp), device_id_type=MESH
            )
            greeted += 1
    pl.semaphore_wait(barrier, greeted)

    sends = []

    depth, width = wmod.shape
    if cond_ref.shape[1] == depth:
        own = cond_ref[...]
    else:
        own = cond_ref[:, pl.ds(pl.multiple_of(sp * depth, depth), depth)]
    activated = silu(own.astype(F32)).astype(BF16)
    loads[0].wait()
    mslots[sp] = jnp.dot(activated, wmod[...], preferred_element_type=F32)
    first = []
    for d in range(1, n_sp):
        copy = remote(
            mslots.at[sp], mslots.at[sp], m1_s.at[d], m1_r.at[d], ((sp + d) % n_sp, tp)
        )
        copy.start()
        first.append(copy)
    sends += first

    decay_copies = []
    for d in range(1, group):
        copy = remote(
            dec_ref, dec_all.at[sub], dec_s.at[d], dec_r.at[d],
            (zz * group + (sub + d) % group, tp),
        )
        copy.start()
        decay_copies.append(copy)
    sends += decay_copies
    dec_all[sub] = dec_ref[...]

    lat_copies = []
    for d in range(1, chips):
        copy = remote(
            lat_ref, lat_all.at[me], lat_s.at[d], lat_r.at[d],
            member_device(((chip + d) % chips) * CORES + core),
        )
        copy.start()
        lat_copies.append(copy)
    sends += lat_copies
    own_relay = remote(lat_ref, lat_all.at[me], rel_s.at[0], rel_r.at[0], partner)
    own_relay.start()
    relays = [own_relay]
    lat_all[me] = lat_ref[...]

    ends = sorted({0, nz - 1})
    ctx_sends = []
    for e in ends:
        for s in range(group):
            dest = e * group + s
            slot = len(ctx_sends)

            def ctx_copy(dest=dest, slot=slot):
                return remote(ctx_ref, ctx_all.at[sp], ctx_s.at[slot], ctx_r.at[sp], (dest, tp))

            @pl.when(sp != dest)
            def _(ctx_copy=ctx_copy):
                ctx_copy().start()

            ctx_sends.append((dest, ctx_copy))
    ctx_all[sp] = ctx_ref[...]

    for copy in first:
        copy.wait_recv()
    total = mslots[0]
    for s in range(1, n_sp):
        total = total + mslots[s]
    mod_cols = pl.ds(pl.multiple_of(tp * width, width), width)
    modfull[:, mod_cols] = total
    second = []
    for d in range(1, n_tp):
        copy = remote(
            modfull.at[:, mod_cols], modfull.at[:, mod_cols], m2_s.at[d], m2_r.at[d],
            (sp, (tp + d) % n_tp),
        )
        copy.start()
        second.append(copy)
    sends += second

    for copy in decay_copies:
        copy.wait_recv()
    head = sub if head_count > 1 else 0
    parts = [dec_all[s, pl.ds(head, 1), :] for s in range(group)]
    a_row = parts[0] if group == 1 else jnp.concatenate(parts, axis=1)
    ii = lax.broadcasted_iota(jnp.int32, (tokens, tokens), 0)
    jj = lax.broadcasted_iota(jnp.int32, (tokens, tokens), 1)
    a_full = jnp.broadcast_to(a_row, (tokens, tokens))
    b_col = jnp.sum(jnp.where(jj <= ii, a_full, 0.0), axis=1, keepdims=True)
    a_col = jnp.sum(jnp.where(jj == ii, a_full, 0.0), axis=1, keepdims=True)
    c_col = b_col - a_col
    b_row = jnp.sum(jnp.where(jj == ii, b_col, 0.0), axis=0, keepdims=True)
    c_row = jnp.sum(jnp.where(jj == ii, c_col, 0.0), axis=0, keepdims=True)
    gap = jnp.where(jj <= ii, b_col - b_row, c_row - c_col)
    wdec[...] = jnp.where(jj == ii, 2.0, jnp.exp(jnp.minimum(gap, 0.0)))
    t_all = b_col[tokens - 1 : tokens, :]
    vecs[0] = jnp.exp(b_col)
    vecs[1] = jnp.exp(t_all - c_col)
    vecs[2] = jnp.exp(t_all - b_col)
    vecs[3] = jnp.exp(c_col)
    etot[...] = jnp.broadcast_to(jnp.exp(t_all), etot.shape)

    for d in range(1, chips):
        lat_copies[d - 1].wait_recv()
        source = ((chip + chips - d) % chips) * CORES + core
        copy = remote(lat_all.at[source], lat_all.at[source], rel_s.at[d], rel_r.at[d], partner)
        copy.start()
        relays.append(copy)
    sends += relays

    for copy in second:
        copy.wait_recv()
    for copy in relays:
        copy.wait_recv()

    gain = ngain_ref[...]

    def modulate(x, row):
        wide = x.astype(F32)
        normal = wide * lax.rsqrt(jnp.mean(wide * wide, axis=-1, keepdims=True) + epsilon)
        shift = modfull[row : row + 1, 0:model]
        scale = modfull[row : row + 1, model : 2 * model]
        return (normal * gain * (1.0 + scale) + shift).astype(BF16)

    @pl.loop(0, members)
    def _(m):
        normed[m] = modulate(lat_all[m], 0)

    x = normed[...].reshape(tokens, model)
    lanes = lax.broadcasted_iota(jnp.int32, (GRID_W, DK // 2), 1)
    even = lanes % 2 == 0
    row_base = zz * (tokens // GRID_W)

    def rotate_into(dst, scale):
        for r in range(tokens // GRID_W):
            at = slice(r * GRID_W, (r + 1) * GRID_W)
            row_c = rowc_ref[pl.ds(row_base + r, 1), :]
            row_s = rows_ref[pl.ds(row_base + r, 1), :]
            for part in range(2):
                cut = slice(part * (DK // 2), (part + 1) * (DK // 2))
                u = ybuf[at, cut]
                swapped = jnp.where(
                    even, pltpu.roll(u, DK // 2 - 1, 1), pltpu.roll(u, 1, 1)
                )
                if part == 0:
                    turned = u * row_c + swapped * row_s
                else:
                    turned = u * colc_ref[...] + swapped * cols_ref[...]
                dst[at, cut] = (turned * scale).astype(BF16)

    loads[1].wait()
    ybuf[:, 0:DK] = jnp.dot(x, wk[...], preferred_element_type=F32)
    rotate_into(kbuf, DK ** (-0.5))
    loads[2].wait()
    for n in range(DV // 256):
        cut = slice(n * 256, (n + 1) * 256)
        vbuf[:, cut] = jnp.dot(x, wv[:, cut], preferred_element_type=F32).astype(BF16)

    over_tokens = (((0,), (0,)), ((), ()))

    @pl.when((zz == 0) | (zz == nz - 1))
    def _():
        for s in range(n_sp):
            @pl.when(sp != s)
            def _(s=s):
                remote(
                    ctx_ref, ctx_all.at[s], ctx_s.at[0], ctx_r.at[s], (sp, tp)
                ).wait_recv()
        cn = modulate(ctx_all[...].reshape(-1, model), 1)
        ck = (jnp.dot(cn, wk[...], preferred_element_type=F32) * DK ** (-0.5)).astype(BF16)
        cv = jnp.dot(cn, wv[...], preferred_element_type=F32).astype(BF16)
        state = lax.dot_general(ck, cv, over_tokens, preferred_element_type=F32) * float(CTX_LIFT)
        state = state.astype(BF16).reshape(recv_f.shape)

        @pl.when(zz == 0)
        def _():
            recv_f[...] = state

        @pl.when(zz == nz - 1)
        def _():
            recv_b[...] = state

    v = vbuf[...]
    kw = kbuf[...].astype(F32)
    fstate[...] = lax.dot_general(
        (kw * vecs[2]).astype(BF16), v, over_tokens, preferred_element_type=F32
    )
    bstate[...] = lax.dot_general(
        (kw * vecs[3]).astype(BF16), v, over_tokens, preferred_element_type=F32
    )

    piece = DK // CHUNKS

    def f_copy(c):
        return remote(
            send_f.at[c], recv_f.at[c], f_s.at[c], f_r.at[c], ((sp + group) % n_sp, tp)
        )

    def b_copy(c):
        return remote(
            send_b.at[c], recv_b.at[c], b_s.at[c], b_r.at[c], ((sp + n_sp - group) % n_sp, tp)
        )

    def chain_f():
        for c in range(CHUNKS):
            @pl.when(zz > 0)
            def _(c=c):
                f_copy(c).wait_recv()

            @pl.when(zz < nz - 1)
            def _(c=c):
                cut = slice(c * piece, (c + 1) * piece)
                send_f[c] = (etot[...] * recv_f[c].astype(F32) + fstate[cut, :]).astype(BF16)
                f_copy(c).start()

    def chain_b():
        for c in range(CHUNKS):
            @pl.when(zz < nz - 1)
            def _(c=c):
                b_copy(c).wait_recv()

            @pl.when(zz > 0)
            def _(c=c):
                cut = slice(c * piece, (c + 1) * piece)
                send_b[c] = (etot[...] * recv_b[c].astype(F32) + bstate[cut, :]).astype(BF16)
                b_copy(c).start()

    @pl.when(2 * zz < nz)
    def _():
        chain_f()

    @pl.when(2 * zz >= nz)
    def _():
        chain_b()

    loads[3].wait()
    ybuf[:, 0:DK] = jnp.dot(x, wq[...], preferred_element_type=F32)
    rotate_into(qbuf, 1.0)
    q = qbuf[...]
    scores = lax.dot_general(
        q, kbuf[...], (((1,), (1,)), ((), ())), preferred_element_type=F32
    )
    ybuf[...] = jnp.dot((scores * wdec[...]).astype(BF16), v, preferred_element_type=F32)

    @pl.when(2 * zz < nz)
    def _():
        chain_b()

    @pl.when(2 * zz >= nz)
    def _():
        chain_f()

    loads[4].wait()
    for n in range(DV // 256):
        cut = slice(n * 256, (n + 1) * 256)
        g = jnp.dot(x, wg[:, cut], preferred_element_type=F32).astype(BF16)
        gbuf[:, cut] = silu(g.astype(F32)) * ggain_ref[
            :, pl.ds(pl.multiple_of(sub * DV + n * 256, 256), 256)
        ]

    y = ybuf[...]
    y = y + vecs[0] * jnp.dot(q, recv_f[...].reshape(DK, DV), preferred_element_type=F32)
    y = y + vecs[1] * jnp.dot(q, recv_b[...].reshape(DK, DV), preferred_element_type=F32)
    ybuf[...] = y

    @pl.loop(0, chips)
    def _(c):
        span = CORES * rows
        at = pl.ds(pl.multiple_of(c * span, span), span)
        part = ybuf[at, :]
        centred = part - jnp.mean(part, axis=-1, keepdims=True)
        variance = jnp.mean(centred * centred, axis=-1, keepdims=True)
        att[c] = (gbuf[at, :] * (centred * lax.rsqrt(variance + epsilon))).astype(BF16)

    loads[5].wait()
    order = list(range(1, chips)) + [0]
    pair_copies = {}
    final = {}

    def finish(d):
        pair_copies[d].wait_recv()
        both = pout[d, core].astype(F32) + pin[d].astype(F32)
        if d == 0:
            final["own"] = both
            return
        psend[d] = both.astype(BF16)
        copy = remote(
            psend.at[d], pfin.at[d], ici_s.at[d], ici_r.at[d],
            member_device(((chip + d) % chips) * CORES + core),
        )
        copy.start()
        final[d] = copy
        sends.append(copy)

    for place, d in enumerate(order):
        rows_of = att[(chip + d) % chips]
        pout[d] = (
            jnp.dot(rows_of, wo[...], preferred_element_type=F32)
            .astype(BF16)
            .reshape(CORES, rows, model)
        )
        copy = remote(pout.at[d, 1 - core], pin.at[d], d2d_s.at[d], d2d_r.at[d], partner)
        copy.start()
        pair_copies[d] = copy
        sends.append(copy)
        if place:
            finish(order[place - 1])
    finish(order[-1])
    acc = final["own"]
    for d in range(1, chips):
        final[d].wait_recv()
        acc = acc + pfin[d].astype(F32)
    gate = modfull[0:1, 2 * model : 3 * model]
    out_ref[...] = (lat_ref[...].astype(F32) + gate * acc).astype(BF16)

    for copy in sends:
        copy.wait_send()
    for dest, ctx_copy in ctx_sends:
        @pl.when(sp != dest)
        def _(ctx_copy=ctx_copy):
            ctx_copy().wait_send()

    @pl.when(zz < nz - 1)
    def _():
        for c in range(CHUNKS):
            f_copy(c).wait_send()

    @pl.when(zz > 0)
    def _():
        for c in range(CHUNKS):
            b_copy(c).wait_send()


def per_device(
    n_sp, n_tp,
    latent, log_decay, context, condition, w_modulate, norm_gain,
    w_query, w_key, w_value, w_gate, group_gain, w_output,
):
    rows, model = latent.shape
    head_count = w_query.shape[1] // DK
    group = head_count
    members = group * n_tp
    chips = members // CORES
    tokens = members * rows
    depth, width = w_modulate.shape
    ctx_rows = context.shape[0]
    if depth % 128:
        condition = lax.dynamic_slice_in_dim(condition, lax.axis_index("sp") * depth, depth, 1)
    total_rows = rows * n_sp * n_tp
    tables = [jnp.asarray(t) for t in rotary_tables(total_rows // GRID_W)]
    vmem = pl.BlockSpec(memory_space=pltpu.VMEM)
    hbm = pl.BlockSpec(memory_space=pl.ANY)
    sem = pltpu.SemaphoreType.DMA
    ends = 2 * group
    scratch = [
        pltpu.VMEM((depth, width), BF16),
        pltpu.VMEM((model, DK), BF16),
        pltpu.VMEM((model, DV), BF16),
        pltpu.VMEM((model, DK), BF16),
        pltpu.VMEM((model, DV), BF16),
        pltpu.VMEM((DV, model), BF16),
        pltpu.VMEM((members, rows, model), BF16),
        pltpu.VMEM((members, rows, model), BF16),
        pltpu.VMEM((n_sp, ctx_rows, model), BF16),
        pltpu.VMEM((group, head_count, log_decay.shape[0]), F32),
        pltpu.VMEM((n_sp, condition.shape[0], width), F32),
        pltpu.VMEM((condition.shape[0], width * n_tp), F32),
        pltpu.VMEM((tokens, tokens), F32),
        pltpu.VMEM((4, tokens, 1), F32),
        pltpu.VMEM((1, DV), F32),
        pltpu.VMEM((tokens, DK), BF16),
        pltpu.VMEM((tokens, DK), BF16),
        pltpu.VMEM((tokens, DV), BF16),
        pltpu.VMEM((tokens, DV), F32),
        pltpu.VMEM((tokens, DV), F32),
        pltpu.VMEM((DK, DV), F32),
        pltpu.VMEM((DK, DV), F32),
        pltpu.VMEM((CHUNKS, DK // CHUNKS, DV), BF16),
        pltpu.VMEM((CHUNKS, DK // CHUNKS, DV), BF16),
        pltpu.VMEM((CHUNKS, DK // CHUNKS, DV), BF16),
        pltpu.VMEM((CHUNKS, DK // CHUNKS, DV), BF16),
        pltpu.VMEM((chips, CORES * rows, DV), BF16),
        pltpu.VMEM((chips, CORES, rows, model), BF16),
        pltpu.VMEM((chips, rows, model), BF16),
        pltpu.VMEM((chips, rows, model), BF16),
        pltpu.VMEM((chips, rows, model), BF16),
        sem((6,)),
        sem((group,)), sem((group,)),
        sem((n_sp,)), sem((n_sp,)),
        sem((n_tp,)), sem((n_tp,)),
        sem((chips,)), sem((chips,)),
        sem((chips,)), sem((chips,)),
        sem((ends,)), sem((n_sp,)),
        sem((CHUNKS,)), sem((CHUNKS,)),
        sem((CHUNKS,)), sem((CHUNKS,)),
        sem((chips,)), sem((chips,)),
        sem((chips,)), sem((chips,)),
    ]
    return pl.pallas_call(
        functools.partial(kernel, n_sp, n_tp, group, rows, head_count),
        out_shape=jax.ShapeDtypeStruct((rows, model), BF16),
        in_specs=[vmem] * 10 + [hbm] * 6,
        out_specs=vmem,
        scratch_shapes=scratch,
        compiler_params=pltpu.CompilerParams(
            collective_id=0, has_side_effects=True, vmem_limit_bytes=58 * 1024 * 1024
        ),
    )(
        latent, log_decay.T, context, condition,
        norm_gain.astype(F32).reshape(1, -1), group_gain.astype(F32).reshape(1, -1),
        *tables,
        w_modulate, w_query, w_key, w_value, w_gate, w_output,
    )


def solution(mesh):
    placed = (
        P(("sp", "tp"), None),
        P("sp", "tp"),
        P("sp", None),
        P(),
        P("sp", "tp"),
        P(),
        P(None, "tp"),
        P(None, "tp"),
        P(None, "tp"),
        P(None, "tp"),
        P("tp"),
        P("tp", None),
    )
    body = functools.partial(per_device, mesh.shape["sp"], mesh.shape["tp"])
    return jax.shard_map(
        body, mesh=mesh, in_specs=placed, out_specs=P(("sp", "tp"), None), check_vma=False
    )
```

time: 446 us -> 74.7 us (0.17)
  waiting for transfers between devices: 175 us -> 0 us
  blocking collectives: 100 us -> 0 us
  Pallas kernels: 0 us -> 70.2 us
  other arithmetic: 61 us -> 2.56 us
  local copies, waits for them, and re-layouts: 52.4 us -> 1.67 us
  matrix products: 39.5 us -> 0 us
  between operations: 14.3 us -> 0.01 us
    all_gather x3 -> x0, waiting for transfers between devices: 152 us -> none  [the longest x2 142 us: carried_in_2(): everything = jax.tree.map(lambda part: lax.all_gather(part, axis), array)]
    pallas_call x0 -> x1, Pallas kernels: none -> 70.2 us  [per_device(): pl.pallas_call(functools.partial(kernel, n_sp, n_tp, group, rows, head_co...]
    dot_general x14 -> x0, matrix products: 39.5 us -> none  [the longest x1 7.35 us: per_device(): jnp.dot(attended, w_output, preferred_element_type=jnp.float32)]
    all_gather x2 -> x0, blocking collectives: 39 us -> none  [the longest x1 33.8 us: per_device(): lax.all_gather(context, 'sp', axis=0, tiled=True)]
    psum x1 -> x0, blocking collectives: 38.9 us -> none  [per_device(): summed = lax.psum(partial_mod, 'sp')]
    select_n x16 -> x0, other arithmetic: 26.1 us -> none  [hop(): return jax.tree.map(lambda a, b: jnp.where(reached, a, b), new, before)]
    reduce_scatter x1 -> x0, waiting for transfers between devices: 23.2 us -> none  [per_device(): lax.psum_scatter(jnp.dot(attended, w_output, preferred_element_type=jnp.f...]
    unnamed x1 -> x0, blocking collectives: 22.6 us -> none
  transfers between devices with their start and end apart: 4 -> 0, of which waited for: 4 -> 0; matrix products, arithmetic and copies ran while one was open for 13% -> 0% of each run, Pallas kernels for 0% -> 0%
where the time goes in v1:
time: 74.7 us; the launch traced here: 74.5 us
  Pallas kernels  70.2 us (94%)
  other arithmetic  2.56 us (3%)
  local copies, waits for them, and re-layouts  1.67 us (2%)
    pallas_call x1, Pallas kernels, per_device(): pl.pallas_call(functools.partial(kernel, n_sp, n_tp, group, rows, head_co...  70.2 us
    unnamed x1, local copies, waits for them, and re-layouts  1.67 us

profile of v1, /device:TPU:0, one launch (start us, length us, event | category | flops | bytes accessed | tf_op | source)
XLA Modules:
  0.0 74.5 jit_solution(289826049304995355)
XLA Ops:
  0.0 1.3 %reshape.16 = f32[1024]{0:T(1024)} convert(bf16[1024]{0:T(1024)(128)(2,1)} %param.26) | non-fusion elementwise | flops 1024 | bytes 6144 | tf_op jit(solution)/shard_map/reshape | solution.py:517
  1.3 1.3 %reshape.14 = f32[2048]{0:T(1024)} convert(bf16[2048]{0:T(1024)(128)(2,1)} %param.21) | non-fusion elementwise | flops 2048 | bytes 12288 | tf_op jit(solution)/shard_map/reshape | solution.py:517
  2.6 70.2 %shard_map.154 = bf16[64,2048]{1,0:T(8,128)(2,1)} custom-call(bf16[64,2048]{1,0:T(8,128)(2,1)} %lat_ref.1, f32[2,256]{1,0:T(2,128)} %bitcast.5, bf16[16,2048]{1,0:T(8,128)(2,1)} %ctx_ref.1, bf16[2,2048]{1,0:T(2,128)(2,1)} %cond_ref.1, f32[1,2048]{1,0:T(1,128)} %bitcast.3, f32[1,1024]{1,0:T(1,128)} %bitcast.4, f32[32,128]{1,0:T(8,128)} %constant.8.clone.rowc_ref, ...), custom_call_target="tpu_custom_call" | custom-call | tf_op jit(solution)/shard_map/pallas_call | solution.py:506
  72.8 1.7 %copy.18 = bf16[64,2048]{1,0:T(8,128)(2,1)} copy(bf16[64,2048]{1,0:T(8,128)(2,1)} %shard_map.154) | data formatting | bytes 524288

commit v2 on v1

--- a/solution.py
+++ b/solution.py
@@ -51,9 +51,9 @@
     wdec, vecs, etot,
     kbuf, qbuf, vbuf, gbuf, ybuf, fstate, bstate,
     recv_f, recv_b, send_f, send_b,
-    att, pout, pin, psend, pfin,
+    pout, pin, psend, pfin,
     w_sem, dec_s, dec_r, m1_s, m1_r, m2_s, m2_r, lat_s, lat_r, rel_s, rel_r,
-    ctx_s, ctx_r, f_s, f_r, b_s, b_r, d2d_s, d2d_r, ici_s, ici_r,
+    ctx_s, ctx_r, ctx_x, f_s, f_r, b_s, b_r, d2d_s, d2d_r, ici_s, ici_r,
 ):
     sp = lax.axis_index("sp")
     tp = lax.axis_index("tp")
@@ -67,6 +67,17 @@
     core = me % CORES
     tokens = members * rows
     model = lat_ref.shape[1]
+    line = chips // group
+    at_line = chip % line
+
+    def peer(k, sign=1):
+        ds, dx = k // line, k % line
+        to_sub = (sub + group + sign * ds) % group
+        return to_sub * line + (at_line + line + sign * dx) % line
+
+    straight = [k for k in range(1, chips) if k % line == 0]
+    across = [k for k in range(1, chips) if k < line]
+    diagonal = [k for k in range(1, chips) if k % line and k >= line]
 
     def member_device(m):
         return (zz * group + m // n_tp, m % n_tp)
@@ -137,21 +148,27 @@
     sends += decay_copies
     dec_all[sub] = dec_ref[...]
 
-    lat_copies = []
-    for d in range(1, chips):
+    lat_copies = {}
+
+    def send_rows(k):
         copy = remote(
-            lat_ref, lat_all.at[me], lat_s.at[d], lat_r.at[d],
-            member_device(((chip + d) % chips) * CORES + core),
+            lat_ref, lat_all.at[me], lat_s.at[k], lat_r.at[k],
+            member_device(peer(k) * CORES + core),
         )
         copy.start()
-        lat_copies.append(copy)
-    sends += lat_copies
+        lat_copies[k] = copy
+        sends.append(copy)
+
+    for k in straight:
+        send_rows(k)
     own_relay = remote(lat_ref, lat_all.at[me], rel_s.at[0], rel_r.at[0], partner)
     own_relay.start()
-    relays = [own_relay]
+    sends.append(own_relay)
     lat_all[me] = lat_ref[...]
 
     ends = sorted({0, nz - 1})
+    half = model // CORES
+    half_cols = pl.ds(pl.multiple_of(core * half, half), half)
     ctx_sends = []
     for e in ends:
         for s in range(group):
@@ -159,14 +176,17 @@
             slot = len(ctx_sends)
 
             def ctx_copy(dest=dest, slot=slot):
-                return remote(ctx_ref, ctx_all.at[sp], ctx_s.at[slot], ctx_r.at[sp], (dest, tp))
+                return remote(
+                    ctx_ref.at[:, half_cols], ctx_all.at[sp, :, half_cols],
+                    ctx_s.at[slot], ctx_r.at[sp], (dest, tp),
+                )
 
             @pl.when(sp != dest)
             def _(ctx_copy=ctx_copy):
                 ctx_copy().start()
 
             ctx_sends.append((dest, ctx_copy))
-    ctx_all[sp] = ctx_ref[...]
+    ctx_all[sp, :, half_cols] = ctx_ref[:, half_cols]
 
     for copy in first:
         copy.wait_recv()
@@ -184,6 +204,8 @@
         copy.start()
         second.append(copy)
     sends += second
+    for k in across + diagonal:
+        send_rows(k)
 
     for copy in decay_copies:
         copy.wait_recv()
@@ -207,20 +229,9 @@
     vecs[3] = jnp.exp(c_col)
     etot[...] = jnp.broadcast_to(jnp.exp(t_all), etot.shape)
 
-    for d in range(1, chips):
-        lat_copies[d - 1].wait_recv()
-        source = ((chip + chips - d) % chips) * CORES + core
-        copy = remote(lat_all.at[source], lat_all.at[source], rel_s.at[d], rel_r.at[d], partner)
-        copy.start()
-        relays.append(copy)
-    sends += relays
-
     for copy in second:
         copy.wait_recv()
-    for copy in relays:
-        copy.wait_recv()
-
-    gain = ngain_ref[...]
+    gain = ngain_ref[...].astype(F32).reshape(1, -1)
 
     def modulate(x, row):
         wide = x.astype(F32)
@@ -229,9 +240,62 @@
         scale = modfull[row : row + 1, model : 2 * model]
         return (normal * gain * (1.0 + scale) + shift).astype(BF16)
 
-    @pl.loop(0, members)
-    def _(m):
+    def normalise(m):
         normed[m] = modulate(lat_all[m], 0)
+
+    def arrive(k):
+        mine = peer(k, -1) * CORES + core
+        other = peer(k, -1) * CORES + (1 - core)
+        relay = own_relay
+        if k:
+            lat_copies[k].wait_recv()
+            relay = remote(lat_all.at[mine], lat_all.at[mine], rel_s.at[k], rel_r.at[k], partner)
+            relay.start()
+            sends.append(relay)
+        normalise(mine)
+        relay.wait_recv()
+        normalise(other)
+
+    for k in [0] + straight + across:
+        arrive(k)
+
+    loads[1].wait()
+    loads[2].wait()
+    over_tokens = (((0,), (0,)), ((), ()))
+    end = (zz == 0) | (zz == nz - 1)
+    lower = 2 * zz < nz
+
+    @pl.when(end)
+    def _():
+        for s in range(n_sp):
+            @pl.when(sp != s)
+            def _(s=s):
+                remote(
+                    ctx_ref.at[:, half_cols], ctx_all.at[s, :, half_cols],
+                    ctx_s.at[0], ctx_r.at[s], partner,
+                ).wait_recv()
+        swap = remote(
+            ctx_all.at[:, :, half_cols], ctx_all.at[:, :, half_cols],
+            ctx_x.at[0], ctx_x.at[1], partner,
+        )
+        swap.start()
+        swap.wait()
+        cn = modulate(ctx_all[...].reshape(-1, model), 1)
+        ck = (jnp.dot(cn, wk[...], preferred_element_type=F32) * DK ** (-0.5)).astype(BF16)
+        cv = jnp.dot(cn, wv[...], preferred_element_type=F32).astype(BF16)
+        state = lax.dot_general(ck, cv, over_tokens, preferred_element_type=F32) * float(CTX_LIFT)
+        state = state.astype(BF16).reshape(recv_f.shape)
+
+        @pl.when(zz == 0)
+        def _():
+            recv_f[...] = state
+
+        @pl.when(zz == nz - 1)
+        def _():
+            recv_b[...] = state
+
+    for k in diagonal:
+        arrive(k)
 
     x = normed[...].reshape(tokens, model)
     lanes = lax.broadcasted_iota(jnp.int32, (GRID_W, DK // 2), 1)
@@ -255,37 +319,11 @@
                     turned = u * colc_ref[...] + swapped * cols_ref[...]
                 dst[at, cut] = (turned * scale).astype(BF16)
 
-    loads[1].wait()
     ybuf[:, 0:DK] = jnp.dot(x, wk[...], preferred_element_type=F32)
     rotate_into(kbuf, DK ** (-0.5))
-    loads[2].wait()
     for n in range(DV // 256):
         cut = slice(n * 256, (n + 1) * 256)
         vbuf[:, cut] = jnp.dot(x, wv[:, cut], preferred_element_type=F32).astype(BF16)
-
-    over_tokens = (((0,), (0,)), ((), ()))
-
-    @pl.when((zz == 0) | (zz == nz - 1))
-    def _():
-        for s in range(n_sp):
-            @pl.when(sp != s)
-            def _(s=s):
-                remote(
-                    ctx_ref, ctx_all.at[s], ctx_s.at[0], ctx_r.at[s], (sp, tp)
-                ).wait_recv()
-        cn = modulate(ctx_all[...].reshape(-1, model), 1)
-        ck = (jnp.dot(cn, wk[...], preferred_element_type=F32) * DK ** (-0.5)).astype(BF16)
-        cv = jnp.dot(cn, wv[...], preferred_element_type=F32).astype(BF16)
-        state = lax.dot_general(ck, cv, over_tokens, preferred_element_type=F32) * float(CTX_LIFT)
-        state = state.astype(BF16).reshape(recv_f.shape)
-
-        @pl.when(zz == 0)
-        def _():
-            recv_f[...] = state
-
-        @pl.when(zz == nz - 1)
-        def _():
-            recv_b[...] = state
 
     v = vbuf[...]
     kw = kbuf[...].astype(F32)
@@ -332,55 +370,40 @@
                 send_b[c] = (etot[...] * recv_b[c].astype(F32) + bstate[cut, :]).astype(BF16)
                 b_copy(c).start()
 
-    @pl.when(2 * zz < nz)
-    def _():
-        chain_f()
-
-    @pl.when(2 * zz >= nz)
-    def _():
-        chain_b()
-
+    def chain(where, forward_if):
+        @pl.when(where & forward_if)
+        def _():
+            chain_f()
+
+        @pl.when(where & jnp.logical_not(forward_if))
+        def _():
+            chain_b()
+
+    middle = jnp.logical_not(end)
+    upper = jnp.logical_not(lower)
+    chain(end, lower)
     loads[3].wait()
     ybuf[:, 0:DK] = jnp.dot(x, wq[...], preferred_element_type=F32)
     rotate_into(qbuf, 1.0)
-    q = qbuf[...]
+    chain(middle, lower)
     scores = lax.dot_general(
-        q, kbuf[...], (((1,), (1,)), ((), ())), preferred_element_type=F32
+        qbuf[...], kbuf[...], (((1,), (1,)), ((), ())), preferred_element_type=F32
     )
     ybuf[...] = jnp.dot((scores * wdec[...]).astype(BF16), v, preferred_element_type=F32)
-
-    @pl.when(2 * zz < nz)
-    def _():
-        chain_b()
-
-    @pl.when(2 * zz >= nz)
-    def _():
-        chain_f()
-
+    chain(middle, upper)
     loads[4].wait()
+    gains = ggain_ref[...].astype(F32).reshape(head_count, DV)
+    group_row = gains[0:1]
+    for h in range(1, head_count):
+        group_row = jnp.where(sub == h, gains[h : h + 1], group_row)
     for n in range(DV // 256):
         cut = slice(n * 256, (n + 1) * 256)
         g = jnp.dot(x, wg[:, cut], preferred_element_type=F32).astype(BF16)
-        gbuf[:, cut] = silu(g.astype(F32)) * ggain_ref[
-            :, pl.ds(pl.multiple_of(sub * DV + n * 256, 256), 256)
-        ]
-
-    y = ybuf[...]
-    y = y + vecs[0] * jnp.dot(q, recv_f[...].reshape(DK, DV), preferred_element_type=F32)
-    y = y + vecs[1] * jnp.dot(q, recv_b[...].reshape(DK, DV), preferred_element_type=F32)
-    ybuf[...] = y
-
-    @pl.loop(0, chips)
-    def _(c):
-        span = CORES * rows
-        at = pl.ds(pl.multiple_of(c * span, span), span)
-        part = ybuf[at, :]
-        centred = part - jnp.mean(part, axis=-1, keepdims=True)
-        variance = jnp.mean(centred * centred, axis=-1, keepdims=True)
-        att[c] = (gbuf[at, :] * (centred * lax.rsqrt(variance + epsilon))).astype(BF16)
+        gbuf[:, cut] = silu(g.astype(F32)) * group_row[:, cut]
+    chain(end, upper)
 
     loads[5].wait()
-    order = list(range(1, chips)) + [0]
+    order = diagonal + across + straight + [0]
     pair_copies = {}
     final = {}
 
@@ -393,14 +416,30 @@
         psend[d] = both.astype(BF16)
         copy = remote(
             psend.at[d], pfin.at[d], ici_s.at[d], ici_r.at[d],
-            member_device(((chip + d) % chips) * CORES + core),
+            member_device(peer(d) * CORES + core),
         )
         copy.start()
         final[d] = copy
         sends.append(copy)
 
+    span = CORES * rows
+
+    def attend(c):
+        at = pl.ds(pl.multiple_of(c * span, span), span)
+        q = qbuf[at, :]
+        y = ybuf[at, :]
+        y = y + vecs[0, at, :] * jnp.dot(
+            q, recv_f[...].reshape(DK, DV), preferred_element_type=F32
+        )
+        y = y + vecs[1, at, :] * jnp.dot(
+            q, recv_b[...].reshape(DK, DV), preferred_element_type=F32
+        )
+        centred = y - jnp.mean(y, axis=-1, keepdims=True)
+        variance = jnp.mean(centred * centred, axis=-1, keepdims=True)
+        return (gbuf[at, :] * (centred * lax.rsqrt(variance + epsilon))).astype(BF16)
+
     for place, d in enumerate(order):
-        rows_of = att[(chip + d) % chips]
+        rows_of = attend(peer(d))
         pout[d] = (
             jnp.dot(rows_of, wo[...], preferred_element_type=F32)
             .astype(BF16)
@@ -486,7 +525,6 @@
         pltpu.VMEM((CHUNKS, DK // CHUNKS, DV), BF16),
         pltpu.VMEM((CHUNKS, DK // CHUNKS, DV), BF16),
         pltpu.VMEM((CHUNKS, DK // CHUNKS, DV), BF16),
-        pltpu.VMEM((chips, CORES * rows, DV), BF16),
         pltpu.VMEM((chips, CORES, rows, model), BF16),
         pltpu.VMEM((chips, rows, model), BF16),
         pltpu.VMEM((chips, rows, model), BF16),
@@ -497,7 +535,7 @@
         sem((n_tp,)), sem((n_tp,)),
         sem((chips,)), sem((chips,)),
         sem((chips,)), sem((chips,)),
-        sem((ends,)), sem((n_sp,)),
+        sem((ends,)), sem((n_sp,)), sem((2,)),
         sem((CHUNKS,)), sem((CHUNKS,)),
         sem((CHUNKS,)), sem((CHUNKS,)),
         sem((chips,)), sem((chips,)),
@@ -514,7 +552,7 @@
         ),
     )(
         latent, log_decay.T, context, condition,
-        norm_gain.astype(F32).reshape(1, -1), group_gain.astype(F32).reshape(1, -1),
+        norm_gain, group_gain,
         *tables,
         w_modulate, w_query, w_key, w_value, w_gate, w_output,
     )

time: 74.7 us -> 66.4 us (0.89)
  Pallas kernels: 70.2 us -> 64.6 us
  other arithmetic: 2.56 us -> 0 us
    pallas_call x1, Pallas kernels: 70.2 us -> 64.6 us  [per_device(): pl.pallas_call(functools.partial(kernel, n_sp, n_tp, group, rows, head_co...]
    reshape x2 -> x0, other arithmetic: 2.56 us -> none  [the longest x1 1.29 us: per_device(): norm_gain.astype(F32).reshape(1, -1)]
where the time goes in v2:
time: 66.4 us; the launch traced here: 66.2 us
  Pallas kernels  64.6 us (97%)
  local copies, waits for them, and re-layouts  1.67 us (3%)
    pallas_call x1, Pallas kernels, per_device(): pl.pallas_call(functools.partial(kernel, n_sp, n_tp, group, rows, head_co...  64.6 us
    unnamed x1, local copies, waits for them, and re-layouts  1.67 us

profile of v2, /device:TPU:0, one launch (start us, length us, event | category | flops | bytes accessed | tf_op | source)
XLA Modules:
  0.0 66.2 jit_solution(6778711906793883779)
XLA Ops:
  0.0 64.6 %shard_map.154 = bf16[64,2048]{1,0:T(8,128)(2,1)} custom-call(bf16[64,2048]{1,0:T(8,128)(2,1)} %lat_ref.1, f32[2,256]{1,0:T(2,128)} %bitcast.1, bf16[16,2048]{1,0:T(8,128)(2,1)} %ctx_ref.1, bf16[2,2048]{1,0:T(2,128)(2,1)} %cond_ref.1, bf16[2048]{0:T(1024)(128)(2,1)} %ngain_ref.1, bf16[1024]{0:T(1024)(128)(2,1)} %ggain_ref.1, ...), custom_call_target="tpu_custom_call" | custom-call | tf_op jit(solution)/shard_map/pallas_call | solution.py:544
  64.6 1.7 %copy.18 = bf16[64,2048]{1,0:T(8,128)(2,1)} copy(bf16[64,2048]{1,0:T(8,128)(2,1)} %shard_map.154) | data formatting | bytes 524288

commit v3 on v2

--- a/solution.py
+++ b/solution.py
@@ -13,7 +13,7 @@
 GRID_W = 64
 CTX_LIFT = 4
 CORES = 2
-CHUNKS = 4
+CHUNKS = 8
 
 epsilon = 1e-06
 rotary_base = 10000.0

time: 66.4 us -> 66.5 us (level)
  no operation moved by 1% of the time
where the time goes in v3:
time: 66.5 us; the launch traced here: 66.4 us
  Pallas kernels  64.7 us (97%)
  local copies, waits for them, and re-layouts  1.67 us (3%)
    pallas_call x1, Pallas kernels, per_device(): pl.pallas_call(functools.partial(kernel, n_sp, n_tp, group, rows, head_co...  64.7 us
    unnamed x1, local copies, waits for them, and re-layouts  1.67 us

profile of v3, /device:TPU:0, one launch (start us, length us, event | category | flops | bytes accessed | tf_op | source)
XLA Modules:
  0.0 66.4 jit_solution(9868131878998402888)
XLA Ops:
  0.0 64.7 %shard_map.154 = bf16[64,2048]{1,0:T(8,128)(2,1)} custom-call(bf16[64,2048]{1,0:T(8,128)(2,1)} %lat_ref.1, f32[2,256]{1,0:T(2,128)} %bitcast.1, bf16[16,2048]{1,0:T(8,128)(2,1)} %ctx_ref.1, bf16[2,2048]{1,0:T(2,128)(2,1)} %cond_ref.1, bf16[2048]{0:T(1024)(128)(2,1)} %ngain_ref.1, bf16[1024]{0:T(1024)(128)(2,1)} %ggain_ref.1, ...), custom_call_target="tpu_custom_call" | custom-call | tf_op jit(solution)/shard_map/pallas_call | solution.py:544
  64.7 1.7 %copy.18 = bf16[64,2048]{1,0:T(8,128)(2,1)} copy(bf16[64,2048]{1,0:T(8,128)(2,1)} %shard_map.154) | data formatting | bytes 524288
